TPU v7x, 32 devices: a whole 2x2x4 slice. The times are simulated.
32 devices in a mesh: kv: 8 (over z, y), tp: 4 (over x, core).
Axes of the slice: x: 2, y: 2, z: 4, core: 2. Of those that a mesh axis runs over, the one named last changes fastest.
Arguments:
- tokens: bfloat16 [8192, 1024], P('kv', 'tp'), may hold values from -6 to 6
- query_weight: bfloat16 [1024, 2048], P(None, 'tp'), may hold values from -0.1875 to 0.1875
- latent_weight: bfloat16 [1024, 128], replicated, may hold values from -0.1875 to 0.1875
- query_gain: float32 [128], replicated, may hold values from 0.5 to 1.5
- key_gain: float32 [128], replicated, may hold values from 0.5 to 1.5
- value_up: bfloat16 [16, 128, 64], P('tp'), may hold values from -0.5 to 0.5
- out_weight: bfloat16 [1024, 1024], P('tp'), may hold values from -0.25 to 0.25
- out_gain: float32 [1024], replicated, may hold values from 0.5 to 1.5
- chosen: int32 [64, 32], P('kv'), may hold values from -1 to 63, as said below
Outputs:
- mixed_out: bfloat16 [8192, 1024], P('kv', 'tp')
Inputs may be any that keep to these rules, and one draw needn't show every extreme that they name: Row b lists the key blocks chosen for query block b: entry 0 is b itself, then distinct blocks before b, then -1 in every unused place. Block j is held by index j // 8 of kv. All query blocks of one index of kv together choose at most 2 distinct blocks held by any one other index, and some pair of indices reaches that bound; blocks held by the same index are chosen freely.
All inputs are finite; a program needn't handle non-finite values.
Results may differ from a plain program's by a relative error of at most 0.02.
Values may be sent and summed in bfloat16 or wider, within the bound.
A program may use at most 64 MiB of HBM per device.

v0:
```python
import jax
import jax.numpy as jnp
from jax import lax
from jax.sharding import PartitionSpec as P

BLOCK = 128
PER_OWNER = 2
epsilon = 1e-06
masked_score = -1e30


def taken_in(shard, axis, dim, absorb, carry):
    whole = jax.tree.map(lambda part: lax.all_gather(part, axis, axis=dim, tiled=True), shard)
    return absorb(carry, whole, jnp.int32(0))


def own_rows(product, rows, axis):
    everything = product(jnp.int32(0), lax.axis_size(axis) * rows)
    own = lax.psum_scatter(everything.astype(jnp.bfloat16), axis, scatter_dimension=0, tiled=True)
    return own.astype(jnp.float32)


def rms_scale(values, gain_row):
    widened = values.astype(jnp.float32)
    mean_sq = jnp.mean(widened * widened, axis=-1, keepdims=True)
    return (widened * lax.rsqrt(mean_sq + epsilon) * gain_row).astype(jnp.bfloat16)


def on_device(
    tokens,
    query_weight,
    latent_weight,
    query_gain,
    key_gain,
    value_up,
    out_weight,
    out_gain,
    chosen,
):
    tok_rows = tokens.shape[0]
    head_cols = query_weight.shape[1]
    lat_width = latent_weight.shape[1]
    local_heads = head_cols // lat_width
    block_size = BLOCK
    blocks_dev = tok_rows // block_size
    owners = lax.axis_size("kv")
    my_owner = lax.axis_index("kv")

    def project(totals, shard_piece, offset):
        query_rows = lax.dynamic_slice_in_dim(query_weight, offset, shard_piece.shape[1], 0)
        latent_rows = lax.dynamic_slice_in_dim(latent_weight, offset, shard_piece.shape[1], 0)
        return (
            totals[0] + jnp.dot(shard_piece, query_rows, preferred_element_type=jnp.float32),
            totals[1] + jnp.dot(shard_piece, latent_rows, preferred_element_type=jnp.float32),
        )

    query_zero = jnp.zeros((tok_rows, head_cols), jnp.float32)
    latent_zero = jnp.zeros((tok_rows, lat_width), jnp.float32)
    query_acc, latent_acc = taken_in(tokens, "tp", 1, project, (query_zero, latent_zero))
    queries = rms_scale(
        query_acc.astype(jnp.bfloat16).reshape(tok_rows, local_heads, lat_width), query_gain
    )
    latent = latent_acc.astype(jnp.bfloat16)
    latent_blocks = latent.reshape(blocks_dev, block_size, lat_width)
    clamped = jnp.maximum(chosen, 0)
    owner_of = clamped // blocks_dev
    index_in = clamped % blocks_dev
    flat_owner = owner_of.reshape(-1)
    flat_index = index_in.reshape(-1)
    remote = (chosen.reshape(-1) >= 0) & (flat_owner != my_owner)
    owner_ids = jnp.arange(owners, dtype=jnp.int32)
    local_ids = jnp.arange(blocks_dev, dtype=jnp.int32)
    matches = (
        remote[:, None, None]
        & (flat_owner[:, None, None] == owner_ids[None, :, None])
        & (flat_index[:, None, None] == local_ids[None, None, :])
    )
    needed = jnp.any(matches, axis=0)
    ranking = jnp.cumsum(needed.astype(jnp.int32), axis=1) - 1
    slot_ids = jnp.arange(PER_OWNER, dtype=jnp.int32)
    placed = needed[:, None, :] & (ranking[:, None, :] == slot_ids[None, :, None])
    wanted = jnp.where(
        jnp.any(placed, axis=2), jnp.sum(jnp.where(placed, local_ids[None, None, :], 0), axis=2), -1
    )
    requested = lax.all_to_all(wanted, "kv", split_axis=0, concat_axis=0, tiled=True)
    served = latent_blocks[jnp.maximum(requested, 0)]
    served = jnp.where((requested >= 0)[:, :, None, None], served, jnp.zeros_like(served))
    arrived = lax.all_to_all(served, "kv", split_axis=0, concat_axis=0, tiled=True)
    block_pool = jnp.concatenate(
        [latent_blocks, arrived.reshape(owners * PER_OWNER, block_size, lat_width)], axis=0
    )
    slot_of = jnp.sum(jnp.where(wanted[owner_of] == index_in[:, :, None], slot_ids, 0), axis=2)
    where_from = jnp.where(
        owner_of == my_owner, index_in, blocks_dev + owner_of * PER_OWNER + slot_of
    )
    selected = block_pool[where_from]
    score_scale = lat_width ** (-0.5)
    offsets = jnp.arange(block_size, dtype=jnp.int32)
    query_blocks = queries.reshape(blocks_dev, block_size, local_heads, lat_width)
    block_starts = my_owner * tok_rows + jnp.arange(blocks_dev, dtype=jnp.int32) * block_size

    def attend(packed):
        query_block, picked_values, chosen_row, start_pos = packed
        picked_keys = rms_scale(picked_values, key_gain)
        scores = (
            jnp.einsum(
                "qhl,ckl->qhck", query_block, picked_keys, preferred_element_type=jnp.float32
            )
            * score_scale
        )
        key_pos = jnp.maximum(chosen_row, 0)[:, None] * block_size + offsets[None, :]
        query_pos = start_pos + offsets
        allowed = (chosen_row[:, None] >= 0)[None] & (key_pos[None] <= query_pos[:, None, None])
        allowed = allowed[:, None]
        scores = jnp.where(allowed, scores, masked_score)
        row_max = jnp.max(scores, axis=(2, 3), keepdims=True)
        exp_scores = jnp.where(allowed, jnp.exp(scores - row_max), 0.0)
        weights = (exp_scores / jnp.sum(exp_scores, axis=(2, 3), keepdims=True)).astype(
            jnp.bfloat16
        )
        attended = jnp.einsum(
            "qhck,ckl->qhl", weights, picked_values, preferred_element_type=jnp.float32
        )
        return attended.astype(jnp.bfloat16)

    attended = lax.map(attend, (query_blocks, selected, chosen, block_starts))
    attended = attended.reshape(tok_rows, local_heads, lat_width)
    heads_out = jnp.einsum("thl,hlv->thv", attended, value_up, preferred_element_type=jnp.float32)
    heads_out = heads_out.astype(jnp.bfloat16).reshape(tok_rows, local_heads * value_up.shape[2])
    model_width = out_weight.shape[1]
    tp_count = lax.axis_size("tp")
    feature_rows = model_width // tp_count
    gain_part = lax.dynamic_slice_in_dim(
        out_gain, lax.axis_index("tp") * feature_rows, feature_rows, 0
    )

    def columns(offset, count):
        weight_cols = lax.dynamic_slice_in_dim(out_weight, offset, count, 1)
        return lax.dot_general(
            weight_cols, heads_out, (((0,), (1,)), ((), ())), preferred_element_type=jnp.float32
        )

    summed = own_rows(columns, feature_rows, "tp").T
    squares = lax.psum(jnp.sum(summed * summed, axis=1), "tp")
    mixed_out = (summed * lax.rsqrt(squares / model_width + epsilon)[:, None] * gain_part).astype(
        jnp.bfloat16
    )
    return mixed_out


def solution(mesh):
    in_specs = (
        P("kv", "tp"),
        P(None, "tp"),
        P(),
        P(),
        P(),
        P("tp", None, None),
        P("tp", None),
        P(),
        P("kv", None),
    )
    out_specs = P("kv", "tp")
    return jax.shard_map(
        on_device, mesh=mesh, in_specs=in_specs, out_specs=out_specs, check_vma=False
    )
```

profile of v0, /device:TPU:0, one launch (start us, length us, event | category | flops | bytes accessed | tf_op | source)
XLA Modules:
  0.0 234.5 jit_solution(9330237730256950675)
XLA Ops:
  10.4 7.3 %all-to-all-start = ((s32[8,1,2]{2,1,0:T(1,128)}), s32[8,1,2]{2,1,0:T(1,128)S(1)}, u32[]{:S(2)}, u32[]{:S(2)}) async-start(s32[8,1,2]{2,1,0:T(1,128)} %bitcast.27), calls=%async_computation | async-start | bytes 8192 | tf_op jit(solution)/shard_map/all_to_all | solution.py:85
  20.3 3.8 %all-to-all-done = s32[8,1,2]{2,1,0:T(1,128)S(1)} async-done(((s32[8,1,2]{2,1,0:T(1,128)}), s32[8,1,2]{2,1,0:T(1,128)S(1)}, u32[]{:S(2)}, u32[]{:S(2)}) %all-to-all-start) | async-done | bytes 96 | tf_op jit(solution)/shard_map/all_to_all | solution.py:85
  24.5 10.0 %all-gather.2.cloned.1.call-done = bf16[1024,1024]{1,0:T(8,128)(2,1)} async-done(((bf16[1024,256]{1,0:T(8,128)(2,1)}), bf16[1024,1024]{1,0:T(8,128)(2,1)}) %all-gather.2.cloned.1.call-update) | async-done | bytes 2097168 | tf_op jit(solution)/shard_map/all_gather | solution.py:13
  34.5 2.3 convolution_convert_fusion.2
  38.3 5.5 %all-to-all-start.1 = ((bf16[8,2,128,128]{3,2,1,0:T(8,128)(2,1)}), bf16[8,2,128,128]{3,2,1,0:T(8,128)(2,1)}, u32[]{:S(2)}, u32[]{:S(2)}) async-start(bf16[8,2,128,128]{3,2,1,0:T(8,128)(2,1)} %broadcast_select_fusion), calls=%async_computation.1 | async-start | bytes 1048576 | tf_op jit(solution)/shard_map/all_to_all | solution.py:88
  43.9 2.9 %bitcast_reduce_fusion = (f32[1024,4]{0,1:T(4,128)S(1)}, bf16[1024,512]{0,1:T(8,128)(2,1)S(1)}) fusion(bf16[1024,1024]{1,0:T(8,128)(2,1)} %all-gather.2.cloned.1.call-done, bf16[1024,512]{1,0:T(8,128)(2,1)S(1)} %copy-done), kind=kOutput, calls=%fused_computation.39 | convolution fusion | flops 1075834880 | bytes 4210688 | tf_op jit(solution)/shard_map/dot_general | solution.py:53
  47.1 1.8 copy.47
  48.9 1.9 copy.32
  50.9 1.6 multiply_convert_fusion.1
  52.4 6.4 %all-to-all-done.1 = bf16[8,2,128,128]{3,2,1,0:T(8,128)(2,1)} async-done(((bf16[8,2,128,128]{3,2,1,0:T(8,128)(2,1)}), bf16[8,2,128,128]{3,2,1,0:T(8,128)(2,1)}, u32[]{:S(2)}, u32[]{:S(2)}) %all-to-all-start.1) | async-done | bytes 524320 | tf_op jit(solution)/shard_map/all_to_all | solution.py:88
  60.0 8.3 %gather_fusion.2 = bf16[256,128,128]{2,1,0:T(8,128)(2,1)} fusion(bf16[24,128,128]{2,1,0:T(8,128)(2,1)S(1)} %pad_maximum_fusion, s32[1024]{0:T(1024)S(1)} %pad_clamp_fusion), kind=kCustom, calls=%fused_computation.2 | custom fusion | bytes 16778240 | tf_op jit(solution)/shard_map/gather | solution.py:96
  68.3 118.1 %while.12 = (s32[]{:T(128)}, bf16[8,128,4,128]{3,1,0,2:T(8,128)(2,1)S(1)}, s32[8,32]{1,0:T(8,128)}, s32[8]{0:T(128)S(1)}, bf16[8,128,4,128]{3,1,2,0:T(8,128)(2,1...) while((s32[]{:T(128)}, ...), condition=%wide.region_10.11_spmd.clone.clone, body=%wide.region_6.10_spmd.clone.clone.sunk | while | flops 1107893504 | bytes 30783664 | solution.py:126
  71.9 1.8 multiply_reduce_fusion.2
  73.7 2.8 %fusion.45 = (f32[128,4]{0,1:T(4,128)S(1)}, f32[128,4,32,128]{0,3,2,1:T(8,128)S(1)}) fusion(pred[128,32,128]{0,2,1:T(8,128)(4,1)S(1)} %compare_and_fusion.3, f32[128]{0:T(128)S(1)} %get-tuple-element.179, f32[32,128]{1,0:T(8,128)S(1)} %add_rsqrt_fusion.3, bf16[8,32,128,128]{3,2,1,0:T(8,128)(2,1)} %get-tuple-element.178, s32[]{:T(128)} %get-tuple-element.165, ...), kind=kOutput, calls=%fused_computation.7.clone.1 | convolution fusion | flops 545259008 | bytes 10112512 | tf_op jit(solution)/shard_map/while/body/eval_jaxpr/qhl,ckl->qhck/dot_general | solution.py:106
  76.5 2.1 fusion.46
  78.6 4.5 %fusion.47 = bf16[8,128,4,128]{3,1,0,2:T(8,128)(2,1)S(1)} fusion(bf16[8,128,4,128]{3,1,0,2:T(8,128)(2,1)S(1)} %get-tuple-element.166, s32[]{:T(128)} %get-tuple-element.165, f32[128,4,32,128]{0,3,2,1:T(8,128)S(1)} %get-tuple-element.155, f32[128,4]{0,1:T(4,128)S(1)} %fusion.46, f32[128,4]{0,1:T(4,128)S(1)} %get-tuple-element.156, ...), kind=kOutput, calls=%fused_computation.16.clone.1 | convolution fusion | flops 549519360 | bytes 10097664 | tf_op jit(solution)/shard_map/while/body/eval_jaxpr/qhck,ckl->qhl/dot_general | solution.py:121
  86.6 1.8 multiply_reduce_fusion.2
  88.5 2.8 %fusion.45 = (f32[128,4]{0,1:T(4,128)S(1)}, f32[128,4,32,128]{0,3,2,1:T(8,128)S(1)}) fusion(pred[128,32,128]{0,2,1:T(8,128)(4,1)S(1)} %compare_and_fusion.3, f32[128]{0:T(128)S(1)} %get-tuple-element.179, f32[32,128]{1,0:T(8,128)S(1)} %add_rsqrt_fusion.3, bf16[8,32,128,128]{3,2,1,0:T(8,128)(2,1)} %get-tuple-element.178, s32[]{:T(128)} %get-tuple-element.165, ...), kind=kOutput, calls=%fused_computation.7.clone.1 | convolution fusion | flops 545259008 | bytes 10112512 | tf_op jit(solution)/shard_map/while/body/eval_jaxpr/qhl,ckl->qhck/dot_general | solution.py:106
  91.3 2.1 fusion.46
  93.4 4.5 %fusion.47 = bf16[8,128,4,128]{3,1,0,2:T(8,128)(2,1)S(1)} fusion(bf16[8,128,4,128]{3,1,0,2:T(8,128)(2,1)S(1)} %get-tuple-element.166, s32[]{:T(128)} %get-tuple-element.165, f32[128,4,32,128]{0,3,2,1:T(8,128)S(1)} %get-tuple-element.155, f32[128,4]{0,1:T(4,128)S(1)} %fusion.46, f32[128,4]{0,1:T(4,128)S(1)} %get-tuple-element.156, ...), kind=kOutput, calls=%fused_computation.16.clone.1 | convolution fusion | flops 549519360 | bytes 10097664 | tf_op jit(solution)/shard_map/while/body/eval_jaxpr/qhck,ckl->qhl/dot_general | solution.py:121
  101.4 1.8 multiply_reduce_fusion.2
  103.3 2.8 %fusion.45 = (f32[128,4]{0,1:T(4,128)S(1)}, f32[128,4,32,128]{0,3,2,1:T(8,128)S(1)}) fusion(pred[128,32,128]{0,2,1:T(8,128)(4,1)S(1)} %compare_and_fusion.3, f32[128]{0:T(128)S(1)} %get-tuple-element.179, f32[32,128]{1,0:T(8,128)S(1)} %add_rsqrt_fusion.3, bf16[8,32,128,128]{3,2,1,0:T(8,128)(2,1)} %get-tuple-element.178, s32[]{:T(128)} %get-tuple-element.165, ...), kind=kOutput, calls=%fused_computation.7.clone.1 | convolution fusion | flops 545259008 | bytes 10112512 | tf_op jit(solution)/shard_map/while/body/eval_jaxpr/qhl,ckl->qhck/dot_general | solution.py:106
  106.0 2.1 fusion.46
  108.1 4.5 %fusion.47 = bf16[8,128,4,128]{3,1,0,2:T(8,128)(2,1)S(1)} fusion(bf16[8,128,4,128]{3,1,0,2:T(8,128)(2,1)S(1)} %get-tuple-element.166, s32[]{:T(128)} %get-tuple-element.165, f32[128,4,32,128]{0,3,2,1:T(8,128)S(1)} %get-tuple-element.155, f32[128,4]{0,1:T(4,128)S(1)} %fusion.46, f32[128,4]{0,1:T(4,128)S(1)} %get-tuple-element.156, ...), kind=kOutput, calls=%fused_computation.16.clone.1 | convolution fusion | flops 549519360 | bytes 10097664 | tf_op jit(solution)/shard_map/while/body/eval_jaxpr/qhck,ckl->qhl/dot_general | solution.py:121
  116.1 1.8 multiply_reduce_fusion.2
  118.0 2.8 %fusion.45 = (f32[128,4]{0,1:T(4,128)S(1)}, f32[128,4,32,128]{0,3,2,1:T(8,128)S(1)}) fusion(pred[128,32,128]{0,2,1:T(8,128)(4,1)S(1)} %compare_and_fusion.3, f32[128]{0:T(128)S(1)} %get-tuple-element.179, f32[32,128]{1,0:T(8,128)S(1)} %add_rsqrt_fusion.3, bf16[8,32,128,128]{3,2,1,0:T(8,128)(2,1)} %get-tuple-element.178, s32[]{:T(128)} %get-tuple-element.165, ...), kind=kOutput, calls=%fused_computation.7.clone.1 | convolution fusion | flops 545259008 | bytes 10112512 | tf_op jit(solution)/shard_map/while/body/eval_jaxpr/qhl,ckl->qhck/dot_general | solution.py:106
  120.8 2.1 fusion.46
  122.9 4.5 %fusion.47 = bf16[8,128,4,128]{3,1,0,2:T(8,128)(2,1)S(1)} fusion(bf16[8,128,4,128]{3,1,0,2:T(8,128)(2,1)S(1)} %get-tuple-element.166, s32[]{:T(128)} %get-tuple-element.165, f32[128,4,32,128]{0,3,2,1:T(8,128)S(1)} %get-tuple-element.155, f32[128,4]{0,1:T(4,128)S(1)} %fusion.46, f32[128,4]{0,1:T(4,128)S(1)} %get-tuple-element.156, ...), kind=kOutput, calls=%fused_computation.16.clone.1 | convolution fusion | flops 549519360 | bytes 10097664 | tf_op jit(solution)/shard_map/while/body/eval_jaxpr/qhck,ckl->qhl/dot_general | solution.py:121
  130.9 1.8 multiply_reduce_fusion.2
  132.8 2.8 %fusion.45 = (f32[128,4]{0,1:T(4,128)S(1)}, f32[128,4,32,128]{0,3,2,1:T(8,128)S(1)}) fusion(pred[128,32,128]{0,2,1:T(8,128)(4,1)S(1)} %compare_and_fusion.3, f32[128]{0:T(128)S(1)} %get-tuple-element.179, f32[32,128]{1,0:T(8,128)S(1)} %add_rsqrt_fusion.3, bf16[8,32,128,128]{3,2,1,0:T(8,128)(2,1)} %get-tuple-element.178, s32[]{:T(128)} %get-tuple-element.165, ...), kind=kOutput, calls=%fused_computation.7.clone.1 | convolution fusion | flops 545259008 | bytes 10112512 | tf_op jit(solution)/shard_map/while/body/eval_jaxpr/qhl,ckl->qhck/dot_general | solution.py:106
  135.6 2.1 fusion.46
  137.7 4.5 %fusion.47 = bf16[8,128,4,128]{3,1,0,2:T(8,128)(2,1)S(1)} fusion(bf16[8,128,4,128]{3,1,0,2:T(8,128)(2,1)S(1)} %get-tuple-element.166, s32[]{:T(128)} %get-tuple-element.165, f32[128,4,32,128]{0,3,2,1:T(8,128)S(1)} %get-tuple-element.155, f32[128,4]{0,1:T(4,128)S(1)} %fusion.46, f32[128,4]{0,1:T(4,128)S(1)} %get-tuple-element.156, ...), kind=kOutput, calls=%fused_computation.16.clone.1 | convolution fusion | flops 549519360 | bytes 10097664 | tf_op jit(solution)/shard_map/while/body/eval_jaxpr/qhck,ckl->qhl/dot_general | solution.py:121
  145.7 1.8 multiply_reduce_fusion.2
  147.5 2.8 %fusion.45 = (f32[128,4]{0,1:T(4,128)S(1)}, f32[128,4,32,128]{0,3,2,1:T(8,128)S(1)}) fusion(pred[128,32,128]{0,2,1:T(8,128)(4,1)S(1)} %compare_and_fusion.3, f32[128]{0:T(128)S(1)} %get-tuple-element.179, f32[32,128]{1,0:T(8,128)S(1)} %add_rsqrt_fusion.3, bf16[8,32,128,128]{3,2,1,0:T(8,128)(2,1)} %get-tuple-element.178, s32[]{:T(128)} %get-tuple-element.165, ...), kind=kOutput, calls=%fused_computation.7.clone.1 | convolution fusion | flops 545259008 | bytes 10112512 | tf_op jit(solution)/shard_map/while/body/eval_jaxpr/qhl,ckl->qhck/dot_general | solution.py:106
  150.3 2.1 fusion.46
  152.4 4.5 %fusion.47 = bf16[8,128,4,128]{3,1,0,2:T(8,128)(2,1)S(1)} fusion(bf16[8,128,4,128]{3,1,0,2:T(8,128)(2,1)S(1)} %get-tuple-element.166, s32[]{:T(128)} %get-tuple-element.165, f32[128,4,32,128]{0,3,2,1:T(8,128)S(1)} %get-tuple-element.155, f32[128,4]{0,1:T(4,128)S(1)} %fusion.46, f32[128,4]{0,1:T(4,128)S(1)} %get-tuple-element.156, ...), kind=kOutput, calls=%fused_computation.16.clone.1 | convolution fusion | flops 549519360 | bytes 10097664 | tf_op jit(solution)/shard_map/while/body/eval_jaxpr/qhck,ckl->qhl/dot_general | solution.py:121
  160.4 1.8 multiply_reduce_fusion.2
  162.3 2.8 %fusion.45 = (f32[128,4]{0,1:T(4,128)S(1)}, f32[128,4,32,128]{0,3,2,1:T(8,128)S(1)}) fusion(pred[128,32,128]{0,2,1:T(8,128)(4,1)S(1)} %compare_and_fusion.3, f32[128]{0:T(128)S(1)} %get-tuple-element.179, f32[32,128]{1,0:T(8,128)S(1)} %add_rsqrt_fusion.3, bf16[8,32,128,128]{3,2,1,0:T(8,128)(2,1)} %get-tuple-element.178, s32[]{:T(128)} %get-tuple-element.165, ...), kind=kOutput, calls=%fused_computation.7.clone.1 | convolution fusion | flops 545259008 | bytes 10112512 | tf_op jit(solution)/shard_map/while/body/eval_jaxpr/qhl,ckl->qhck/dot_general | solution.py:106
  165.1 2.1 fusion.46
  167.2 4.5 %fusion.47 = bf16[8,128,4,128]{3,1,0,2:T(8,128)(2,1)S(1)} fusion(bf16[8,128,4,128]{3,1,0,2:T(8,128)(2,1)S(1)} %get-tuple-element.166, s32[]{:T(128)} %get-tuple-element.165, f32[128,4,32,128]{0,3,2,1:T(8,128)S(1)} %get-tuple-element.155, f32[128,4]{0,1:T(4,128)S(1)} %fusion.46, f32[128,4]{0,1:T(4,128)S(1)} %get-tuple-element.156, ...), kind=kOutput, calls=%fused_computation.16.clone.1 | convolution fusion | flops 549519360 | bytes 10097664 | tf_op jit(solution)/shard_map/while/body/eval_jaxpr/qhck,ckl->qhl/dot_general | solution.py:121
  175.2 1.8 multiply_reduce_fusion.2
  177.1 2.8 %fusion.45 = (f32[128,4]{0,1:T(4,128)S(1)}, f32[128,4,32,128]{0,3,2,1:T(8,128)S(1)}) fusion(pred[128,32,128]{0,2,1:T(8,128)(4,1)S(1)} %compare_and_fusion.3, f32[128]{0:T(128)S(1)} %get-tuple-element.179, f32[32,128]{1,0:T(8,128)S(1)} %add_rsqrt_fusion.3, bf16[8,32,128,128]{3,2,1,0:T(8,128)(2,1)} %get-tuple-element.178, s32[]{:T(128)} %get-tuple-element.165, ...), kind=kOutput, calls=%fused_computation.7.clone.1 | convolution fusion | flops 545259008 | bytes 10112512 | tf_op jit(solution)/shard_map/while/body/eval_jaxpr/qhl,ckl->qhck/dot_general | solution.py:106
  179.9 2.1 fusion.46
  182.0 4.5 %fusion.47 = bf16[8,128,4,128]{3,1,0,2:T(8,128)(2,1)S(1)} fusion(bf16[8,128,4,128]{3,1,0,2:T(8,128)(2,1)S(1)} %get-tuple-element.166, s32[]{:T(128)} %get-tuple-element.165, f32[128,4,32,128]{0,3,2,1:T(8,128)S(1)} %get-tuple-element.155, f32[128,4]{0,1:T(4,128)S(1)} %fusion.46, f32[128,4]{0,1:T(4,128)S(1)} %get-tuple-element.156, ...), kind=kOutput, calls=%fused_computation.16.clone.1 | convolution fusion | flops 549519360 | bytes 10097664 | tf_op jit(solution)/shard_map/while/body/eval_jaxpr/qhck,ckl->qhl/dot_general | solution.py:121
  187.0 2.1 convert_bitcast_fusion.1
  189.9 28.7 %reduce-scatter.2.cloned.1.call-done = bf16[256,1024]{0,1:T(8,128)(2,1)} async-done(((bf16[1024,1024]{0,1:T(8,128)(2,1)}), bf16[256,1024]{0,1:T(8,128)(2,1)}) %reduce-scatter.2.cloned.1.call-update) | async-done | bytes 524304 | tf_op jit(solution)/shard_map/reduce_scatter | solution.py:19
  219.8 5.8 %psum.7 = f32[1024]{0:T(1024)S(1)} all-reduce(f32[1024]{0:T(1024)S(1)} %fusion.24), channel_id=1, replica_groups=mesh['kv'=8,'tp'=4] {'tp'}, use_global_device_ids=true, to_apply=%region_13.14 | all-reduce | flops 1024 | bytes 8192 | tf_op jit(solution)/shard_map/psum | solution.py:144
  225.6 2.0 fusion.27
  (112 shorter events, 40.2 us)
Async XLA Ops:
  6.5 37.4 %copy-start = (bf16[1024,512]{1,0:T(8,128)(2,1)S(1)}, bf16[1024,512]{1,0:T(8,128)(2,1)}, u32[]{:S(2)}) copy-start(bf16[1024,512]{1,0:T(8,128)(2,1)} %param.12) | copy-start | bytes 3145732
  6.5 27.9 %all-gather.2.cloned.1.call-start = ((), (), s32[]{:S(2)}) async-start(), calls=%async_computation.3 | async-start | bytes 2621440 | tf_op jit(solution)/shard_map/all_gather | solution.py:13
  10.4 13.7 %all-to-all-start = ((s32[8,1,2]{2,1,0:T(1,128)}), s32[8,1,2]{2,1,0:T(1,128)S(1)}, u32[]{:S(2)}, u32[]{:S(2)}) async-start(s32[8,1,2]{2,1,0:T(1,128)} %bitcast.27), calls=%async_computation | async-start | bytes 8192 | tf_op jit(solution)/shard_map/all_to_all | solution.py:85
  38.3 20.5 %all-to-all-start.1 = ((bf16[8,2,128,128]{3,2,1,0:T(8,128)(2,1)}), bf16[8,2,128,128]{3,2,1,0:T(8,128)(2,1)}, u32[]{:S(2)}, u32[]{:S(2)}) async-start(bf16[8,2,128,128]{3,2,1,0:T(8,128)(2,1)} %broadcast_select_fusion), calls=%async_computation.1 | async-start | bytes 1048576 | tf_op jit(solution)/shard_map/all_to_all | solution.py:88
  43.8 7.0 %copy-start.4 = (f32[128]{0:T(128)S(1)}, f32[128]{0:T(128)}, u32[]{:S(2)}) copy-start(f32[128]{0:T(128)} %param.14) | copy-start | bytes 1540
  43.9 174.7 %reduce-scatter.2.cloned.1.call-start = ((), (), s32[]{:S(2)}) async-start(), calls=%async_computation.4 | async-start | bytes 2621440 | tf_op jit(solution)/shard_map/reduce_scatter | solution.py:19
  60.0 8.3 %copy-start.1 = (bf16[8,128,4,128]{3,1,0,2:T(8,128)(2,1)S(1)}, bf16[8,128,4,128]{3,1,0,2:T(8,128)(2,1)}, u32[]{:S(2)}) copy-start(bf16[8,128,4,128]{3,1,0,2:T(8,128)(2,1)} %custom-call.6) | copy-start | bytes 3145732
  60.0 8.3 %copy-start.5 = (f32[128]{0:T(128)S(1)}, f32[128]{0:T(128)}, u32[]{:S(2)}) copy-start(f32[128]{0:T(128)} %param.15) | copy-start | bytes 1540
  68.3 118.2 %copy-start.3 = (bf16[4,128,64]{1,2,0:T(8,128)(2,1)S(1)}, bf16[4,128,64]{1,2,0:T(8,128)(2,1)}, u32[]{:S(2)}) copy-start(bf16[4,128,64]{1,2,0:T(8,128)(2,1)} %param.16) | copy-start | bytes 196612
  68.3 118.7 %copy-start.2 = (bf16[256,1024]{1,0:T(8,128)(2,1)S(1)}, bf16[256,1024]{1,0:T(8,128)(2,1)}, u32[]{:S(2)}) copy-start(bf16[256,1024]{1,0:T(8,128)(2,1)} %param.17) | copy-start | bytes 1572868
Sparse Core Ops, SparseCore 0:
  8.9 25.5 all-gather.1
  189.2 29.3 reduce-scatter.1
where the time goes:
time: 236 us; the launch traced here: 234 us
  matrix products  66 us (28%)
  other arithmetic  65.6 us (28%)
  waiting for transfers between devices  49.7 us (21%)
  local copies, waits for them, and re-layouts  20.4 us (9%)
  between operations  13.6 us (6%)
  starting transfers between devices  12.9 us (5%)
  blocking collectives  5.77 us (2%)
    dot_general x8, matrix products, attend(): jnp.einsum('qhck,ckl->qhl', weights, picked_values, preferred_element_typ...  35.9 us
    reduce_scatter x1, waiting for transfers between devices, own_rows(): lax.psum_scatter(everything.astype(jnp.bfloat16), axis, scatter_dimension...  28.7 us
    dot_general x8, matrix products, attend(): jnp.einsum('qhl,ckl->qhck', query_block, picked_keys, preferred_element_t...  22.3 us
    reduce_sum x8, other arithmetic, attend(): jnp.sum(exp_scores, axis=(2, 3), keepdims=True)  16.7 us
    reduce_sum x8, other arithmetic, rms_scale(): mean_sq = jnp.mean(widened * widened, axis=-1, keepdims=True)  14.7 us
    all_gather x1, waiting for transfers between devices, taken_in(): lax.all_gather(part, axis, axis=dim, tiled=True)  9.99 us
    gather x1, local copies, waits for them, and re-layouts, on_device(): selected = block_pool[where_from]  8.29 us
    all_to_all x1, starting transfers between devices, on_device(): lax.all_to_all(wanted, 'kv', split_axis=0, concat_axis=0, tiled=True)  7.31 us
  transfers between devices with their start and end apart: 4, of which 4 were waited for; matrix products, arithmetic and copies ran while one was open for 7% of the time, Pallas kernels for 0%

commit v1 on v0

--- a/solution.py
+++ b/solution.py
@@ -85,7 +85,21 @@
     requested = lax.all_to_all(wanted, "kv", split_axis=0, concat_axis=0, tiled=True)
     served = latent_blocks[jnp.maximum(requested, 0)]
     served = jnp.where((requested >= 0)[:, :, None, None], served, jnp.zeros_like(served))
-    arrived = lax.all_to_all(served, "kv", split_axis=0, concat_axis=0, tiled=True)
+    passed, x_next = (lax.axis_size("kv"), lax.axis_index("kv"))
+    inter = served.shape[0] // passed
+    built = list(served.shape)
+    built[0] = inter
+    z = built[0]
+    built[0] = z * passed
+    arrived = jnp.zeros(built, served.dtype)
+    for k0 in tuple(range(passed)):
+        after = lax.dynamic_slice_in_dim(served, (x_next ^ k0) * inter, inter, axis=0)
+        if k0:
+            series = []
+            for pp in [*range(passed)]:
+                series.append((pp, pp ^ k0))
+            after = lax.ppermute(after, "kv", series)
+        arrived = lax.dynamic_update_slice_in_dim(arrived, after, (x_next ^ k0) * z, axis=0)
     block_pool = jnp.concatenate(
         [latent_blocks, arrived.reshape(owners * PER_OWNER, block_size, lat_width)], axis=0
     )

time: 236 us -> 248 us (1.051)
  local copies, waits for them, and re-layouts: 20.4 us -> 30.7 us
  starting transfers between devices: 12.9 us -> 18.5 us
  waiting for transfers between devices: 49.7 us -> 45.1 us
    ppermute x0 -> x7, starting transfers between devices: none -> 11.1 us  [on_device(): after = lax.ppermute(after, 'kv', series)]
    dynamic_update_slice x0 -> x7, local copies, waits for them, and re-layouts: none -> 8.63 us  [on_device(): lax.dynamic_update_slice_in_dim(arrived, after, (x_next ^ k0) * z, axis=0)]
    all_to_all x1 -> x0, waiting for transfers between devices: 6.42 us -> none  [on_device(): lax.all_to_all(served, 'kv', split_axis=0, concat_axis=0, tiled=True)]
    all_to_all x1 -> x0, starting transfers between devices: 5.54 us -> none  [on_device(): lax.all_to_all(served, 'kv', split_axis=0, concat_axis=0, tiled=True)]
  transfers between devices with their start and end apart: 4 -> 10, of which waited for: 4 -> 3; matrix products, arithmetic and copies ran while one was open for 7% -> 10% of each run, Pallas kernels for 0% -> 0%
where the time goes in v1:
time: 248 us; the launch traced here: 246 us
  matrix products  66.6 us (27%)
  other arithmetic  65.5 us (26%)
  waiting for transfers between devices  45.1 us (18%)
  local copies, waits for them, and re-layouts  30.7 us (12%)
  starting transfers between devices  18.5 us (7%)
  between operations  13.6 us (5%)
  blocking collectives  5.77 us (2%)
    dot_general x8, matrix products, attend(): jnp.einsum('qhck,ckl->qhl', weights, picked_values, preferred_element_typ...  35.9 us
    reduce_scatter x1, waiting for transfers between devices, own_rows(): lax.psum_scatter(everything.astype(jnp.bfloat16), axis, scatter_dimension...  30.6 us
    dot_general x8, matrix products, attend(): jnp.einsum('qhl,ckl->qhck', query_block, picked_keys, preferred_element_t...  22.3 us
    reduce_sum x8, other arithmetic, attend(): jnp.sum(exp_scores, axis=(2, 3), keepdims=True)  16.7 us
    reduce_sum x8, other arithmetic, rms_scale(): mean_sq = jnp.mean(widened * widened, axis=-1, keepdims=True)  14.7 us
    ppermute x7, starting transfers between devices, on_device(): after = lax.ppermute(after, 'kv', series)  11.1 us
    all_gather x1, waiting for transfers between devices, taken_in(): lax.all_gather(part, axis, axis=dim, tiled=True)  9.99 us
    dynamic_update_slice x7, local copies, waits for them, and re-layouts, on_device(): lax.dynamic_update_slice_in_dim(arrived, after, (x_next ^ k0) * z, axis=0)  8.63 us
  transfers between devices with their start and end apart: 10, of which 3 were waited for; matrix products, arithmetic and copies ran while one was open for 10% of the time, Pallas kernels for 0%

profile of v1, /device:TPU:0, one launch (start us, length us, event | category | flops | bytes accessed | tf_op | source)
XLA Modules:
  0.0 246.2 jit_solution(18083606361809649599)
XLA Ops:
  10.4 7.3 %all-to-all-start = ((s32[8,1,2]{2,1,0:T(1,128)}), s32[8,1,2]{2,1,0:T(1,128)S(1)}, u32[]{:S(2)}, u32[]{:S(2)}) async-start(s32[8,1,2]{2,1,0:T(1,128)} %bitcast.27), calls=%async_computation | async-start | bytes 8192 | tf_op jit(solution)/shard_map/all_to_all | solution.py:85
  20.4 3.7 %all-to-all-done = s32[8,1,2]{2,1,0:T(1,128)S(1)} async-done(((s32[8,1,2]{2,1,0:T(1,128)}), s32[8,1,2]{2,1,0:T(1,128)S(1)}, u32[]{:S(2)}, u32[]{:S(2)}) %all-to-all-start) | async-done | bytes 96 | tf_op jit(solution)/shard_map/all_to_all | solution.py:85
  24.5 10.0 %all-gather.2.cloned.1.call-done = bf16[1024,1024]{1,0:T(8,128)(2,1)} async-done(((bf16[1024,256]{1,0:T(8,128)(2,1)}), bf16[1024,1024]{1,0:T(8,128)(2,1)}) %all-gather.2.cloned.1.call-update) | async-done | bytes 2097168 | tf_op jit(solution)/shard_map/all_gather | solution.py:13
  34.5 2.3 convolution_convert_fusion.2
  42.7 2.4 collective-permute-start.3
  46.5 3.5 %bitcast_reduce_fusion = (f32[1024,4]{0,1:T(4,128)}, bf16[1024,512]{0,1:T(8,128)(2,1)S(1)}) fusion(bf16[1024,1024]{1,0:T(8,128)(2,1)} %all-gather.2.cloned.1.call-done, bf16[1024,512]{1,0:T(8,128)(2,1)S(1)} %copy-done), kind=kOutput, calls=%fused_computation.39 | convolution fusion | flops 1075834880 | bytes 4210688 | tf_op jit(solution)/shard_map/dot_general | solution.py:53
  50.3 1.8 copy.47
  52.1 1.9 copy.32
  54.8 1.5 multiply_convert_fusion.1
  56.3 3.3 %collective-permute-start.5 = (bf16[1,2,128,128]{3,2,1,0:T(8,128)(2,1)S(1)}, bf16[1,2,128,128]{3,2,1,0:T(8,128)(2,1)S(1)}, u32[]{:S(2)}, u32[]{:S(2)}) collective-permute-start(bf16[1,2,128,128]{3,2,1,0:T(8,128)(2,1)S(1)} %get-tuple-element.104), channel_id=1, source_target_pairs={{0,24},{4,28},{8,16},{12,20},{16,8},{20,12},{24,0},{28,4},{1,25},{... | collective-permute-start | bytes 196616 | tf_op jit(solution)/shard_map/ppermute | solution.py:101
  69.9 8.3 %gather_fusion.2 = bf16[256,128,128]{2,1,0:T(8,128)(2,1)} fusion(bf16[24,128,128]{2,1,0:T(8,128)(2,1)S(1)} %pad_maximum_fusion, s32[1024]{0:T(1024)S(1)} %pad_clamp_fusion), kind=kCustom, calls=%fused_computation.2 | custom fusion | bytes 16778240 | tf_op jit(solution)/shard_map/gather | solution.py:110
  78.2 118.2 %while.12 = (s32[]{:T(128)}, bf16[8,128,4,128]{3,1,0,2:T(8,128)(2,1)S(1)}, s32[8,32]{1,0:T(8,128)}, s32[8]{0:T(128)S(1)}, bf16[8,128,4,128]{3,1,2,0:T(8,128)(2,1...) while((s32[]{:T(128)}, ...), condition=%wide.region_10.11_spmd.clone.clone, body=%wide.region_6.10_spmd.clone.clone.sunk | while | flops 1107893504 | bytes 30783664 | solution.py:140
  81.7 1.8 multiply_reduce_fusion.2
  83.6 2.8 %fusion.45 = (f32[128,4]{0,1:T(4,128)S(1)}, f32[128,4,32,128]{0,3,2,1:T(8,128)S(1)}) fusion(pred[128,32,128]{0,2,1:T(8,128)(4,1)S(1)} %compare_and_fusion.3, f32[128]{0:T(128)S(1)} %get-tuple-element.187, f32[32,128]{1,0:T(8,128)S(1)} %add_rsqrt_fusion.3, bf16[8,32,128,128]{3,2,1,0:T(8,128)(2,1)} %get-tuple-element.186, s32[]{:T(128)} %get-tuple-element.173, ...), kind=kOutput, calls=%fused_computation.7.clone.1 | convolution fusion | flops 545259008 | bytes 10112512 | tf_op jit(solution)/shard_map/while/body/eval_jaxpr/qhl,ckl->qhck/dot_general | solution.py:120
  86.4 2.1 fusion.46
  88.5 4.5 %fusion.47 = bf16[8,128,4,128]{3,1,0,2:T(8,128)(2,1)S(1)} fusion(bf16[8,128,4,128]{3,1,0,2:T(8,128)(2,1)S(1)} %get-tuple-element.174, s32[]{:T(128)} %get-tuple-element.173, f32[128,4,32,128]{0,3,2,1:T(8,128)S(1)} %get-tuple-element.163, f32[128,4]{0,1:T(4,128)S(1)} %fusion.46, f32[128,4]{0,1:T(4,128)S(1)} %get-tuple-element.164, ...), kind=kOutput, calls=%fused_computation.16.clone.1 | convolution fusion | flops 549519360 | bytes 10097664 | tf_op jit(solution)/shard_map/while/body/eval_jaxpr/qhck,ckl->qhl/dot_general | solution.py:135
  96.5 1.8 multiply_reduce_fusion.2
  98.4 2.8 %fusion.45 = (f32[128,4]{0,1:T(4,128)S(1)}, f32[128,4,32,128]{0,3,2,1:T(8,128)S(1)}) fusion(pred[128,32,128]{0,2,1:T(8,128)(4,1)S(1)} %compare_and_fusion.3, f32[128]{0:T(128)S(1)} %get-tuple-element.187, f32[32,128]{1,0:T(8,128)S(1)} %add_rsqrt_fusion.3, bf16[8,32,128,128]{3,2,1,0:T(8,128)(2,1)} %get-tuple-element.186, s32[]{:T(128)} %get-tuple-element.173, ...), kind=kOutput, calls=%fused_computation.7.clone.1 | convolution fusion | flops 545259008 | bytes 10112512 | tf_op jit(solution)/shard_map/while/body/eval_jaxpr/qhl,ckl->qhck/dot_general | solution.py:120
  101.2 2.1 fusion.46
  103.3 4.5 %fusion.47 = bf16[8,128,4,128]{3,1,0,2:T(8,128)(2,1)S(1)} fusion(bf16[8,128,4,128]{3,1,0,2:T(8,128)(2,1)S(1)} %get-tuple-element.174, s32[]{:T(128)} %get-tuple-element.173, f32[128,4,32,128]{0,3,2,1:T(8,128)S(1)} %get-tuple-element.163, f32[128,4]{0,1:T(4,128)S(1)} %fusion.46, f32[128,4]{0,1:T(4,128)S(1)} %get-tuple-element.164, ...), kind=kOutput, calls=%fused_computation.16.clone.1 | convolution fusion | flops 549519360 | bytes 10097664 | tf_op jit(solution)/shard_map/while/body/eval_jaxpr/qhck,ckl->qhl/dot_general | solution.py:135
  111.3 1.8 multiply_reduce_fusion.2
  113.1 2.8 %fusion.45 = (f32[128,4]{0,1:T(4,128)S(1)}, f32[128,4,32,128]{0,3,2,1:T(8,128)S(1)}) fusion(pred[128,32,128]{0,2,1:T(8,128)(4,1)S(1)} %compare_and_fusion.3, f32[128]{0:T(128)S(1)} %get-tuple-element.187, f32[32,128]{1,0:T(8,128)S(1)} %add_rsqrt_fusion.3, bf16[8,32,128,128]{3,2,1,0:T(8,128)(2,1)} %get-tuple-element.186, s32[]{:T(128)} %get-tuple-element.173, ...), kind=kOutput, calls=%fused_computation.7.clone.1 | convolution fusion | flops 545259008 | bytes 10112512 | tf_op jit(solution)/shard_map/while/body/eval_jaxpr/qhl,ckl->qhck/dot_general | solution.py:120
  115.9 2.1 fusion.46
  118.0 4.5 %fusion.47 = bf16[8,128,4,128]{3,1,0,2:T(8,128)(2,1)S(1)} fusion(bf16[8,128,4,128]{3,1,0,2:T(8,128)(2,1)S(1)} %get-tuple-element.174, s32[]{:T(128)} %get-tuple-element.173, f32[128,4,32,128]{0,3,2,1:T(8,128)S(1)} %get-tuple-element.163, f32[128,4]{0,1:T(4,128)S(1)} %fusion.46, f32[128,4]{0,1:T(4,128)S(1)} %get-tuple-element.164, ...), kind=kOutput, calls=%fused_computation.16.clone.1 | convolution fusion | flops 549519360 | bytes 10097664 | tf_op jit(solution)/shard_map/while/body/eval_jaxpr/qhck,ckl->qhl/dot_general | solution.py:135
  126.0 1.8 multiply_reduce_fusion.2
  127.9 2.8 %fusion.45 = (f32[128,4]{0,1:T(4,128)S(1)}, f32[128,4,32,128]{0,3,2,1:T(8,128)S(1)}) fusion(pred[128,32,128]{0,2,1:T(8,128)(4,1)S(1)} %compare_and_fusion.3, f32[128]{0:T(128)S(1)} %get-tuple-element.187, f32[32,128]{1,0:T(8,128)S(1)} %add_rsqrt_fusion.3, bf16[8,32,128,128]{3,2,1,0:T(8,128)(2,1)} %get-tuple-element.186, s32[]{:T(128)} %get-tuple-element.173, ...), kind=kOutput, calls=%fused_computation.7.clone.1 | convolution fusion | flops 545259008 | bytes 10112512 | tf_op jit(solution)/shard_map/while/body/eval_jaxpr/qhl,ckl->qhck/dot_general | solution.py:120
  130.7 2.1 fusion.46
  132.8 4.5 %fusion.47 = bf16[8,128,4,128]{3,1,0,2:T(8,128)(2,1)S(1)} fusion(bf16[8,128,4,128]{3,1,0,2:T(8,128)(2,1)S(1)} %get-tuple-element.174, s32[]{:T(128)} %get-tuple-element.173, f32[128,4,32,128]{0,3,2,1:T(8,128)S(1)} %get-tuple-element.163, f32[128,4]{0,1:T(4,128)S(1)} %fusion.46, f32[128,4]{0,1:T(4,128)S(1)} %get-tuple-element.164, ...), kind=kOutput, calls=%fused_computation.16.clone.1 | convolution fusion | flops 549519360 | bytes 10097664 | tf_op jit(solution)/shard_map/while/body/eval_jaxpr/qhck,ckl->qhl/dot_general | solution.py:135
  140.8 1.8 multiply_reduce_fusion.2
  142.7 2.8 %fusion.45 = (f32[128,4]{0,1:T(4,128)S(1)}, f32[128,4,32,128]{0,3,2,1:T(8,128)S(1)}) fusion(pred[128,32,128]{0,2,1:T(8,128)(4,1)S(1)} %compare_and_fusion.3, f32[128]{0:T(128)S(1)} %get-tuple-element.187, f32[32,128]{1,0:T(8,128)S(1)} %add_rsqrt_fusion.3, bf16[8,32,128,128]{3,2,1,0:T(8,128)(2,1)} %get-tuple-element.186, s32[]{:T(128)} %get-tuple-element.173, ...), kind=kOutput, calls=%fused_computation.7.clone.1 | convolution fusion | flops 545259008 | bytes 10112512 | tf_op jit(solution)/shard_map/while/body/eval_jaxpr/qhl,ckl->qhck/dot_general | solution.py:120
  145.5 2.1 fusion.46
  147.5 4.5 %fusion.47 = bf16[8,128,4,128]{3,1,0,2:T(8,128)(2,1)S(1)} fusion(bf16[8,128,4,128]{3,1,0,2:T(8,128)(2,1)S(1)} %get-tuple-element.174, s32[]{:T(128)} %get-tuple-element.173, f32[128,4,32,128]{0,3,2,1:T(8,128)S(1)} %get-tuple-element.163, f32[128,4]{0,1:T(4,128)S(1)} %fusion.46, f32[128,4]{0,1:T(4,128)S(1)} %get-tuple-element.164, ...), kind=kOutput, calls=%fused_computation.16.clone.1 | convolution fusion | flops 549519360 | bytes 10097664 | tf_op jit(solution)/shard_map/while/body/eval_jaxpr/qhck,ckl->qhl/dot_general | solution.py:135
  155.6 1.8 multiply_reduce_fusion.2
  157.4 2.8 %fusion.45 = (f32[128,4]{0,1:T(4,128)S(1)}, f32[128,4,32,128]{0,3,2,1:T(8,128)S(1)}) fusion(pred[128,32,128]{0,2,1:T(8,128)(4,1)S(1)} %compare_and_fusion.3, f32[128]{0:T(128)S(1)} %get-tuple-element.187, f32[32,128]{1,0:T(8,128)S(1)} %add_rsqrt_fusion.3, bf16[8,32,128,128]{3,2,1,0:T(8,128)(2,1)} %get-tuple-element.186, s32[]{:T(128)} %get-tuple-element.173, ...), kind=kOutput, calls=%fused_computation.7.clone.1 | convolution fusion | flops 545259008 | bytes 10112512 | tf_op jit(solution)/shard_map/while/body/eval_jaxpr/qhl,ckl->qhck/dot_general | solution.py:120
  160.2 2.1 fusion.46
  162.3 4.5 %fusion.47 = bf16[8,128,4,128]{3,1,0,2:T(8,128)(2,1)S(1)} fusion(bf16[8,128,4,128]{3,1,0,2:T(8,128)(2,1)S(1)} %get-tuple-element.174, s32[]{:T(128)} %get-tuple-element.173, f32[128,4,32,128]{0,3,2,1:T(8,128)S(1)} %get-tuple-element.163, f32[128,4]{0,1:T(4,128)S(1)} %fusion.46, f32[128,4]{0,1:T(4,128)S(1)} %get-tuple-element.164, ...), kind=kOutput, calls=%fused_computation.16.clone.1 | convolution fusion | flops 549519360 | bytes 10097664 | tf_op jit(solution)/shard_map/while/body/eval_jaxpr/qhck,ckl->qhl/dot_general | solution.py:135
  170.3 1.8 multiply_reduce_fusion.2
  172.2 2.8 %fusion.45 = (f32[128,4]{0,1:T(4,128)S(1)}, f32[128,4,32,128]{0,3,2,1:T(8,128)S(1)}) fusion(pred[128,32,128]{0,2,1:T(8,128)(4,1)S(1)} %compare_and_fusion.3, f32[128]{0:T(128)S(1)} %get-tuple-element.187, f32[32,128]{1,0:T(8,128)S(1)} %add_rsqrt_fusion.3, bf16[8,32,128,128]{3,2,1,0:T(8,128)(2,1)} %get-tuple-element.186, s32[]{:T(128)} %get-tuple-element.173, ...), kind=kOutput, calls=%fused_computation.7.clone.1 | convolution fusion | flops 545259008 | bytes 10112512 | tf_op jit(solution)/shard_map/while/body/eval_jaxpr/qhl,ckl->qhck/dot_general | solution.py:120
  175.0 2.1 fusion.46
  177.1 4.5 %fusion.47 = bf16[8,128,4,128]{3,1,0,2:T(8,128)(2,1)S(1)} fusion(bf16[8,128,4,128]{3,1,0,2:T(8,128)(2,1)S(1)} %get-tuple-element.174, s32[]{:T(128)} %get-tuple-element.173, f32[128,4,32,128]{0,3,2,1:T(8,128)S(1)} %get-tuple-element.163, f32[128,4]{0,1:T(4,128)S(1)} %fusion.46, f32[128,4]{0,1:T(4,128)S(1)} %get-tuple-element.164, ...), kind=kOutput, calls=%fused_computation.16.clone.1 | convolution fusion | flops 549519360 | bytes 10097664 | tf_op jit(solution)/shard_map/while/body/eval_jaxpr/qhck,ckl->qhl/dot_general | solution.py:135
  185.1 1.8 multiply_reduce_fusion.2
  186.9 2.8 %fusion.45 = (f32[128,4]{0,1:T(4,128)S(1)}, f32[128,4,32,128]{0,3,2,1:T(8,128)S(1)}) fusion(pred[128,32,128]{0,2,1:T(8,128)(4,1)S(1)} %compare_and_fusion.3, f32[128]{0:T(128)S(1)} %get-tuple-element.187, f32[32,128]{1,0:T(8,128)S(1)} %add_rsqrt_fusion.3, bf16[8,32,128,128]{3,2,1,0:T(8,128)(2,1)} %get-tuple-element.186, s32[]{:T(128)} %get-tuple-element.173, ...), kind=kOutput, calls=%fused_computation.7.clone.1 | convolution fusion | flops 545259008 | bytes 10112512 | tf_op jit(solution)/shard_map/while/body/eval_jaxpr/qhl,ckl->qhck/dot_general | solution.py:120
  189.7 2.1 fusion.46
  191.8 4.5 %fusion.47 = bf16[8,128,4,128]{3,1,0,2:T(8,128)(2,1)S(1)} fusion(bf16[8,128,4,128]{3,1,0,2:T(8,128)(2,1)S(1)} %get-tuple-element.174, s32[]{:T(128)} %get-tuple-element.173, f32[128,4,32,128]{0,3,2,1:T(8,128)S(1)} %get-tuple-element.163, f32[128,4]{0,1:T(4,128)S(1)} %fusion.46, f32[128,4]{0,1:T(4,128)S(1)} %get-tuple-element.164, ...), kind=kOutput, calls=%fused_computation.16.clone.1 | convolution fusion | flops 549519360 | bytes 10097664 | tf_op jit(solution)/shard_map/while/body/eval_jaxpr/qhck,ckl->qhl/dot_general | solution.py:135
  196.8 2.1 convert_bitcast_fusion.1
  199.7 30.6 %reduce-scatter.2.cloned.1.call-done = bf16[256,1024]{0,1:T(8,128)(2,1)} async-done(((bf16[1024,1024]{0,1:T(8,128)(2,1)}), bf16[256,1024]{0,1:T(8,128)(2,1)}) %reduce-scatter.2.cloned.1.call-update) | async-done | bytes 524304 | tf_op jit(solution)/shard_map/reduce_scatter | solution.py:19
  231.6 5.8 %psum.7 = f32[1024]{0:T(1024)S(1)} all-reduce(f32[1024]{0:T(1024)S(1)} %fusion.24), channel_id=1, replica_groups=mesh['kv'=8,'tp'=4] {'tp'}, use_global_device_ids=true, to_apply=%region_13.14 | all-reduce | flops 1024 | bytes 8192 | tf_op jit(solution)/shard_map/psum | solution.py:158
  237.4 2.0 fusion.27
  (133 shorter events, 55.8 us)
Async XLA Ops:
  6.5 40.0 %copy-start = (bf16[1024,512]{1,0:T(8,128)(2,1)S(1)}, bf16[1024,512]{1,0:T(8,128)(2,1)}, u32[]{:S(2)}) copy-start(bf16[1024,512]{1,0:T(8,128)(2,1)} %param.12) | copy-start | bytes 3145732
  6.5 27.9 %all-gather.2.cloned.1.call-start = ((), (), s32[]{:S(2)}) async-start(), calls=%async_computation.2 | async-start | bytes 2621440 | tf_op jit(solution)/shard_map/all_gather | solution.py:13
  10.4 13.7 %all-to-all-start = ((s32[8,1,2]{2,1,0:T(1,128)}), s32[8,1,2]{2,1,0:T(1,128)S(1)}, u32[]{:S(2)}, u32[]{:S(2)}) async-start(s32[8,1,2]{2,1,0:T(1,128)} %bitcast.27), calls=%async_computation | async-start | bytes 8192 | tf_op jit(solution)/shard_map/all_to_all | solution.py:85
  17.7 212.6 %reduce-scatter.2.cloned.1.call-start = ((), (), s32[]{:S(2)}) async-start(), calls=%async_computation.3 | async-start | bytes 2621440 | tf_op jit(solution)/shard_map/reduce_scatter | solution.py:19
  39.2 17.1 %collective-permute-start = (bf16[1,2,128,128]{3,2,1,0:T(8,128)(2,1)}, bf16[1,2,128,128]{3,2,1,0:T(8,128)(2,1)}, u32[]{:S(2)}, u32[]{:S(2)}) collective-permute-start(bf16[1,2,128,128]{3,2,1,0:T(8,128)(2,1)} %get-tuple-element.109), channel_id=1, source_target_pairs={{0,4},{4,0},{8,12},{12,8},{16,20},{20,16},{24,28},{28,24},{1,5},{5... | collective-permute-start | bytes 196616 | tf_op jit(solution)/shard_map/ppermute | solution.py:101
  40.6 20.4 %collective-permute-start.1 = (bf16[1,2,128,128]{3,2,1,0:T(8,128)(2,1)}, bf16[1,2,128,128]{3,2,1,0:T(8,128)(2,1)}, u32[]{:S(2)}, u32[]{:S(2)}) collective-permute-start(bf16[1,2,128,128]{3,2,1,0:T(8,128)(2,1)} %get-tuple-element.108), channel_id=1, source_target_pairs={{0,8},{4,12},{8,0},{12,4},{16,24},{20,28},{24,16},{28,20},{1,9},{5... | collective-permute-start | bytes 196616 | tf_op jit(solution)/shard_map/ppermute | solution.py:101
  42.1 20.9 %collective-permute-start.2 = (bf16[1,2,128,128]{3,2,1,0:T(8,128)(2,1)}, bf16[1,2,128,128]{3,2,1,0:T(8,128)(2,1)}, u32[]{:S(2)}, u32[]{:S(2)}) collective-permute-start(bf16[1,2,128,128]{3,2,1,0:T(8,128)(2,1)} %get-tuple-element.107), channel_id=1, source_target_pairs={{0,12},{4,8},{8,4},{12,0},{16,28},{20,24},{24,20},{28,16},{1,13},{... | collective-permute-start | bytes 196616 | tf_op jit(solution)/shard_map/ppermute | solution.py:101
  42.7 21.8 %collective-permute-start.3 = (bf16[1,2,128,128]{3,2,1,0:T(8,128)(2,1)}, bf16[1,2,128,128]{3,2,1,0:T(8,128)(2,1)}, u32[]{:S(2)}, u32[]{:S(2)}) collective-permute-start(bf16[1,2,128,128]{3,2,1,0:T(8,128)(2,1)} %get-tuple-element.106), channel_id=1, source_target_pairs={{0,16},{4,20},{8,24},{12,28},{16,0},{20,4},{24,8},{28,12},{1,17},{... | collective-permute-start | bytes 196616 | tf_op jit(solution)/shard_map/ppermute | solution.py:101
  45.1 9.7 %copy-start.4 = (f32[128]{0:T(128)S(1)}, f32[128]{0:T(128)}, u32[]{:S(2)}) copy-start(f32[128]{0:T(128)} %param.14) | copy-start | bytes 1540
  45.1 20.9 %collective-permute-start.4 = (bf16[1,2,128,128]{3,2,1,0:T(8,128)(2,1)}, bf16[1,2,128,128]{3,2,1,0:T(8,128)(2,1)}, u32[]{:S(2)}, u32[]{:S(2)}) collective-permute-start(bf16[1,2,128,128]{3,2,1,0:T(8,128)(2,1)} %get-tuple-element.105), channel_id=1, source_target_pairs={{0,20},{4,16},{8,28},{12,24},{16,4},{20,0},{24,12},{28,8},{1,21},{... | collective-permute-start | bytes 196616 | tf_op jit(solution)/shard_map/ppermute | solution.py:101
  56.3 11.2 %collective-permute-start.5 = (bf16[1,2,128,128]{3,2,1,0:T(8,128)(2,1)S(1)}, bf16[1,2,128,128]{3,2,1,0:T(8,128)(2,1)S(1)}, u32[]{:S(2)}, u32[]{:S(2)}) collective-permute-start(bf16[1,2,128,128]{3,2,1,0:T(8,128)(2,1)S(1)} %get-tuple-element.104), channel_id=1, source_target_pairs={{0,24},{4,28},{8,16},{12,20},{16,8},{20,12},{24,0},{28,4},{1,25},{... | collective-permute-start | bytes 196616 | tf_op jit(solution)/shard_map/ppermute | solution.py:101
  61.1 7.0 %collective-permute-start.6 = (bf16[1,2,128,128]{3,2,1,0:T(8,128)(2,1)S(1)}, bf16[1,2,128,128]{3,2,1,0:T(8,128)(2,1)S(1)}, u32[]{:S(2)}, u32[]{:S(2)}) collective-permute-start(bf16[1,2,128,128]{3,2,1,0:T(8,128)(2,1)S(1)} %get-tuple-element.103), channel_id=1, source_target_pairs={{0,28},{4,24},{8,20},{12,16},{16,12},{20,8},{24,4},{28,0},{1,29},{... | collective-permute-start | bytes 196616 | tf_op jit(solution)/shard_map/ppermute | solution.py:101
  69.8 8.3 %copy-start.1 = (bf16[8,128,4,128]{3,1,0,2:T(8,128)(2,1)S(1)}, bf16[8,128,4,128]{3,1,0,2:T(8,128)(2,1)}, u32[]{:S(2)}) copy-start(bf16[8,128,4,128]{3,1,0,2:T(8,128)(2,1)} %custom-call.6) | copy-start | bytes 3145732
  69.8 8.3 %copy-start.5 = (f32[128]{0:T(128)S(1)}, f32[128]{0:T(128)}, u32[]{:S(2)}) copy-start(f32[128]{0:T(128)} %param.15) | copy-start | bytes 1540
  78.2 118.2 %copy-start.3 = (bf16[4,128,64]{1,2,0:T(8,128)(2,1)S(1)}, bf16[4,128,64]{1,2,0:T(8,128)(2,1)}, u32[]{:S(2)}) copy-start(bf16[4,128,64]{1,2,0:T(8,128)(2,1)} %param.16) | copy-start | bytes 196612
  78.2 118.7 %copy-start.2 = (bf16[256,1024]{1,0:T(8,128)(2,1)S(1)}, bf16[256,1024]{1,0:T(8,128)(2,1)}, u32[]{:S(2)}) copy-start(bf16[256,1024]{1,0:T(8,128)(2,1)} %param.17) | copy-start | bytes 1572868
Sparse Core Ops, SparseCore 0:
  8.9 25.5 all-gather.1
  199.1 31.1 reduce-scatter.1
